TPU v7x, 32 devices: a whole 2x2x4 slice. The times are simulated.
32 devices in a mesh: rep: 2 (over y), fs: 4 (over z), tp: 4 (over x, core).
Axes of the slice: x: 2, y: 2, z: 4, core: 2. Of those that a mesh axis runs over, the one named last changes fastest.
Arguments:
- tokens: bfloat16 [4096, 2048], P(('rep', 'fs')), may hold values from -6 to 6
- norm_gain: float32 [2048], replicated, may hold values from 0.1 to 1.9
- gate_weight: bfloat16 [2048, 5632], P('fs', 'tp'), may hold values from -0.125 to 0.125
- up_weight: bfloat16 [2048, 5632], P('fs', 'tp'), may hold values from -0.125 to 0.125
- down_weight: bfloat16 [5632, 2048], P('tp', 'fs'), may hold values from -0.078125 to 0.078125
Outputs:
- branch_out: bfloat16 [4096, 2048], P(('rep', 'fs'))
All inputs are finite; a program needn't handle non-finite values.
Results may differ from a plain program's by a relative error of at most 0.014.
Values may be sent and summed in bfloat16 or wider, within the bound.
A program may use at most 64 MiB of HBM per device.

v0:
```python
import jax
import jax.numpy as jnp
from jax import lax
from jax.sharding import PartitionSpec as P


def add_rows(left, piece):
    return jnp.dot(left, piece, preferred_element_type=jnp.float32)


def per_device(tokens, norm_gain, gate_weight, up_weight, down_weight):
    wide_tok = tokens.astype(jnp.float32)
    scale = lax.rsqrt(jnp.mean(wide_tok * wide_tok, axis=-1, keepdims=True) + 1e-06)
    normed = (wide_tok * scale * norm_gain).astype(jnp.bfloat16)

    def add_one(piece):
        return add_rows(normed, piece)

    gate = add_one(lax.all_gather(gate_weight, "fs", axis=0, tiled=True))
    up = add_one(lax.all_gather(up_weight, "fs", axis=0, tiled=True))
    hidden = (jax.nn.silu(gate) * up).astype(jnp.bfloat16)
    partial_value = jnp.dot(
        hidden,
        lax.all_gather(down_weight, "fs", axis=1, tiled=True),
        preferred_element_type=jnp.float32,
    )
    return lax.psum(partial_value.astype(jnp.bfloat16), "tp")


def solution(mesh):
    in_specs = (P(("rep", "fs"), None), P(), P("fs", "tp"), P("fs", "tp"), P("tp", "fs"))
    out_specs = P(("rep", "fs"), None)
    return jax.shard_map(
        per_device, mesh=mesh, in_specs=in_specs, out_specs=out_specs, check_vma=False
    )
```

profile of v0, /device:TPU:0, one launch (start us, length us, event | category | flops | bytes accessed | tf_op | source)
XLA Modules:
  0.0 404.2 jit_solution(18413360618791287892)
XLA Ops:
  6.5 0.0 copy-start
  6.5 0.0 copy-start.1
  6.5 0.0 all-gather.4.cloned.1.call-start
  6.5 0.7 all-gather.4.cloned.1.call-update
  7.3 0.0 all-gather.6.cloned.1.call-start
  7.3 0.7 all-gather.6.cloned.1.call-update
  8.0 0.0 all-gather.8.cloned.1.call-start
  8.1 0.7 all-gather.8.cloned.1.call-update
  8.7 0.0 all-reduce.2.cloned.1.call-start
  8.8 0.0 copy-done
  8.8 0.5 fusion
  9.3 109.1 %all-gather.4.cloned.1.call-done = bf16[2048,1408]{1,0:T(8,128)(2,1)} async-done(((bf16[512,1408]{1,0:T(8,128)(2,1)}), bf16[2048,1408]{1,0:T(8,128)(2,1)}) %all-gather.4.cloned.1.call-update) | async-done | bytes 5767184 | tf_op jit(solution)/shard_map/all_gather | solution.py:19
  118.3 0.0 copy-done.1
  118.4 7.6 %fusion.6 = f32[512,1408]{1,0:T(8,128)} fusion(bf16[2048,1408]{1,0:T(8,128)(2,1)} %all-gather.4.cloned.1.call-done, bf16[512,2048]{1,0:T(8,128)(2,1)S(1)} %copy-done, f32[2048]{0:T(1024)S(1)} %copy-done.1, f32[512]{0:T(512)S(1)} %add_rsqrt_fusion), kind=kOutput, calls=%fused_computation.8 | convolution fusion | flops 2956984320 | bytes 10758144 | tf_op jit(solution)/shard_map/dot_general | solution.py:8
  126.0 98.9 %all-gather.6.cloned.1.call-done = bf16[2048,1408]{1,0:T(8,128)(2,1)} async-done(((bf16[512,1408]{1,0:T(8,128)(2,1)}), bf16[2048,1408]{1,0:T(8,128)(2,1)}) %all-gather.6.cloned.1.call-update) | async-done | bytes 5767184 | tf_op jit(solution)/shard_map/all_gather | solution.py:20
  224.9 106.5 %all-gather.8.cloned.1.call-done = bf16[1408,2048]{1,0:T(8,128)(2,1)} async-done(((bf16[1408,512]{1,0:T(8,128)(2,1)}), bf16[1408,2048]{1,0:T(8,128)(2,1)}) %all-gather.8.cloned.1.call-update) | async-done | bytes 5767184 | tf_op jit(solution)/shard_map/all_gather | solution.py:24
  331.4 13.3 %convolution_convert_fusion = bf16[512,2048]{1,0:T(8,128)(2,1)} fusion(bf16[1408,2048]{1,0:T(8,128)(2,1)} %all-gather.8.cloned.1.call-done, bf16[2048,1408]{1,0:T(8,128)(2,1)} %all-gather.6.cloned.1.call-done, f32[512,1408]{1,0:T(8,128)} %fusion.6, bf16[512,2048]{1,0:T(8,128)(2,1)S(1)} %copy-done, f32[2048]{0:T(1024)S(1)} %copy-done.1, f32[512]{0:T(512)S(1)} %add_rsqrt_fusion), kind=kOutput, calls=%fused_computation.7 | convolution fusion | flops 5915148288 | bytes 18622464 | tf_op jit(solution)/shard_map/dot_general | solution.py:22
  344.7 0.0 all-reduce.2.cloned.1.call-update
  344.7 49.8 %all-reduce.2.cloned.1.call-done = bf16[512,2048]{1,0:T(8,128)(2,1)} async-done(((bf16[512,2048]{1,0:T(8,128)(2,1)}), bf16[512,2048]{1,0:T(8,128)(2,1)}) %all-reduce.2.cloned.1.call-update) | async-done | bytes 2097168 | tf_op jit(solution)/shard_map/psum | solution.py:27
  394.5 3.2 copy.7
  (1 shorter events, 0.0 us)
Async XLA Ops:
  6.5 2.3 copy-start
  6.5 111.8 %copy-start.1 = (f32[2048]{0:T(1024)S(1)}, f32[2048]{0:T(1024)}, u32[]{:S(2)}) copy-start(f32[2048]{0:T(1024)} %param.6) | copy-start | bytes 24580
  6.5 111.8 %all-gather.4.cloned.1.call-start = ((), (), s32[]{:S(2)}) async-start(), calls=%async_computation | async-start | bytes 7208960 | tf_op jit(solution)/shard_map/all_gather | solution.py:19
  7.3 217.6 %all-gather.6.cloned.1.call-start = ((), (), s32[]{:S(2)}) async-start(), calls=%async_computation.1 | async-start | bytes 7208960 | tf_op jit(solution)/shard_map/all_gather | solution.py:20
  8.0 323.4 %all-gather.8.cloned.1.call-start = ((), (), s32[]{:S(2)}) async-start(), calls=%async_computation.2 | async-start | bytes 7208960 | tf_op jit(solution)/shard_map/all_gather | solution.py:24
  8.7 385.8 %all-reduce.2.cloned.1.call-start = ((), (), s32[]{:S(2)}) async-start(), calls=%async_computation.3 | async-start | bytes 4194304 | tf_op jit(solution)/shard_map/psum | solution.py:27
Sparse Core Ops, SparseCore 0:
  8.9 109.3 all-gather.3
  119.9 104.9 all-gather.5
  226.5 104.9 all-gather.7
  344.9 49.6 all-reduce.1
where the time goes:
time: 404 us
  waiting for transfers between devices  366 us (91%)
  matrix products  20.9 us (5%)
  between operations  13.1 us (3%)
    all_gather x1, waiting for transfers between devices, per_device(): gate = add_one(lax.all_gather(gate_weight, 'fs', axis=0, tiled=True))  109 us
    all_gather x1, waiting for transfers between devices, per_device(): lax.all_gather(down_weight, 'fs', axis=1, tiled=True)  107 us
    all_gather x1, waiting for transfers between devices, per_device(): up = add_one(lax.all_gather(up_weight, 'fs', axis=0, tiled=True))  98.9 us
    psum x1, waiting for transfers between devices, per_device(): return lax.psum(partial_value.astype(jnp.bfloat16), 'tp')  49.8 us
    dot_general x1, matrix products, per_device(): jnp.dot(hidden, lax.all_gather(down_weight, 'fs', axis=1, tiled=True), pr...  13.3 us
  transfers between devices with their start and end apart: 4, of which 4 were waited for; matrix products, arithmetic and copies ran while one was open for 2% of the time, Pallas kernels for 0%

commit v1 on v0

--- a/solution.py
+++ b/solution.py
@@ -2,6 +2,11 @@
 import jax.numpy as jnp
 from jax import lax
 from jax.sharding import PartitionSpec as P
+
+
+def summed_here(x, mesh_axis):
+    blocks = lax.all_gather(x, mesh_axis)
+    return jnp.sum(blocks, axis=0)
 
 
 def add_rows(left, piece):
@@ -24,7 +29,7 @@
         lax.all_gather(down_weight, "fs", axis=1, tiled=True),
         preferred_element_type=jnp.float32,
     )
-    return lax.psum(partial_value.astype(jnp.bfloat16), "tp")
+    return summed_here(partial_value.astype(jnp.bfloat16), "tp")
 
 
 def solution(mesh):

time: 404 us -> 415 us (1.027)
  other arithmetic: 0.49 us -> 7.69 us
  waiting for transfers between devices: 366 us -> 373 us
    all_gather x0 -> x1, waiting for transfers between devices: none -> 56.7 us  [summed_here(): blocks = lax.all_gather(x, mesh_axis)]
    psum x1 -> x0, waiting for transfers between devices: 49.8 us -> none  [per_device(): return lax.psum(partial_value.astype(jnp.bfloat16), 'tp')]
    all_gather x1, waiting for transfers between devices: 98.9 us -> 107 us  [per_device(): up = add_one(lax.all_gather(up_weight, 'fs', axis=0, tiled=True))]
    all_gather x1, waiting for transfers between devices: 107 us -> 98.9 us  [per_device(): lax.all_gather(down_weight, 'fs', axis=1, tiled=True)]
    reduce_sum x0 -> x1, other arithmetic: none -> 7.2 us  [summed_here(): return jnp.sum(blocks, axis=0)]
where the time goes in v1:
time: 415 us
  waiting for transfers between devices  373 us (90%)
  matrix products  20.9 us (5%)
  between operations  13.1 us (3%)
  other arithmetic  7.69 us (2%)
    all_gather x1, waiting for transfers between devices, per_device(): gate = add_one(lax.all_gather(gate_weight, 'fs', axis=0, tiled=True))  109 us
    all_gather x1, waiting for transfers between devices, per_device(): up = add_one(lax.all_gather(up_weight, 'fs', axis=0, tiled=True))  107 us
    all_gather x1, waiting for transfers between devices, per_device(): lax.all_gather(down_weight, 'fs', axis=1, tiled=True)  98.9 us
    all_gather x1, waiting for transfers between devices, summed_here(): blocks = lax.all_gather(x, mesh_axis)  56.7 us
    dot_general x1, matrix products, per_device(): jnp.dot(hidden, lax.all_gather(down_weight, 'fs', axis=1, tiled=True), pr...  13.3 us
  transfers between devices with their start and end apart: 4, of which 4 were waited for; matrix products, arithmetic and copies ran while one was open for 2% of the time, Pallas kernels for 0%

profile of v1, /device:TPU:0, one launch (start us, length us, event | category | flops | bytes accessed | tf_op | source)
XLA Modules:
  0.0 415.2 jit_solution(5861046165614172538)
XLA Ops:
  6.5 0.0 copy-start
  6.5 0.0 copy-start.1
  6.5 0.0 all-gather.6.cloned.1.call-start
  6.5 0.7 all-gather.6.cloned.1.call-update
  7.3 0.0 all-gather.10.cloned.1.call-start
  7.3 0.7 all-gather.10.cloned.1.call-update
  8.0 0.0 all-gather.8.cloned.1.call-start
  8.1 0.7 all-gather.8.cloned.1.call-update
  8.7 0.0 all-gather.12.cloned.1.call-start
  8.8 0.0 copy-done
  8.8 0.5 fusion
  9.3 109.1 %all-gather.6.cloned.1.call-done = bf16[2048,1408]{1,0:T(8,128)(2,1)} async-done(((bf16[512,1408]{1,0:T(8,128)(2,1)}), bf16[2048,1408]{1,0:T(8,128)(2,1)}) %all-gather.6.cloned.1.call-update) | async-done | bytes 5767184 | tf_op jit(solution)/shard_map/all_gather | solution.py:24
  118.3 0.0 copy-done.1
  118.4 7.6 %fusion.6 = f32[512,1408]{1,0:T(8,128)} fusion(bf16[2048,1408]{1,0:T(8,128)(2,1)} %all-gather.6.cloned.1.call-done, bf16[512,2048]{1,0:T(8,128)(2,1)S(1)} %copy-done, f32[2048]{0:T(1024)S(1)} %copy-done.1, f32[512]{0:T(512)S(1)} %add_rsqrt_fusion), kind=kOutput, calls=%fused_computation.8 | convolution fusion | flops 2956984320 | bytes 10758144 | tf_op jit(solution)/shard_map/dot_general | solution.py:13
  126.0 98.9 %all-gather.10.cloned.1.call-done = bf16[1408,2048]{1,0:T(8,128)(2,1)} async-done(((bf16[1408,512]{1,0:T(8,128)(2,1)}), bf16[1408,2048]{1,0:T(8,128)(2,1)}) %all-gather.10.cloned.1.call-update) | async-done | bytes 5767184 | tf_op jit(solution)/shard_map/all_gather | solution.py:29
  224.9 106.5 %all-gather.8.cloned.1.call-done = bf16[2048,1408]{1,0:T(8,128)(2,1)} async-done(((bf16[512,1408]{1,0:T(8,128)(2,1)}), bf16[2048,1408]{1,0:T(8,128)(2,1)}) %all-gather.8.cloned.1.call-update) | async-done | bytes 5767184 | tf_op jit(solution)/shard_map/all_gather | solution.py:25
  331.4 13.3 %convolution_convert_fusion = bf16[512,2048]{1,0:T(8,128)(2,1)} fusion(bf16[1408,2048]{1,0:T(8,128)(2,1)} %all-gather.10.cloned.1.call-done, bf16[2048,1408]{1,0:T(8,128)(2,1)} %all-gather.8.cloned.1.call-done, f32[512,1408]{1,0:T(8,128)} %fusion.6, bf16[512,2048]{1,0:T(8,128)(2,1)S(1)} %copy-done, f32[2048]{0:T(1024)S(1)} %copy-done.1, ...), kind=kOutput, calls=%fused_computation.7 | convolution fusion | flops 5915148288 | bytes 18622464 | tf_op jit(solution)/shard_map/dot_general | solution.py:27
  344.7 0.0 all-gather.12.cloned.1.call-update
  344.8 56.7 %all-gather.12.cloned.1.call-done = bf16[2048,2048]{1,0:T(8,128)(2,1)} async-done(((bf16[512,2048]{1,0:T(8,128)(2,1)}), bf16[2048,2048]{1,0:T(8,128)(2,1)}) %all-gather.12.cloned.1.call-update) | async-done | bytes 8388624 | tf_op jit(solution)/shard_map/all_gather | solution.py:8
  401.4 7.2 %reduce_sum.22 = bf16[512,2048]{1,0:T(8,128)(2,1)} reduce(bf16[4,512,2048]{2,1,0:T(8,128)(2,1)} %bitcast.4, bf16[]{:T(256)} %constant.11.clone.1), dimensions={0}, to_apply=%region_1.2 | reduce | flops 3145728 | bytes 10485762 | tf_op jit(solution)/shard_map/reduce_sum | solution.py:9
  (1 shorter events, 0.0 us)
Async XLA Ops:
  6.5 2.3 copy-start
  6.5 111.8 %copy-start.1 = (f32[2048]{0:T(1024)S(1)}, f32[2048]{0:T(1024)}, u32[]{:S(2)}) copy-start(f32[2048]{0:T(1024)} %param.6) | copy-start | bytes 24580
  6.5 111.8 %all-gather.6.cloned.1.call-start = ((), (), s32[]{:S(2)}) async-start(), calls=%async_computation | async-start | bytes 7208960 | tf_op jit(solution)/shard_map/all_gather | solution.py:24
  7.3 217.6 %all-gather.10.cloned.1.call-start = ((), (), s32[]{:S(2)}) async-start(), calls=%async_computation.2 | async-start | bytes 7208960 | tf_op jit(solution)/shard_map/all_gather | solution.py:29
  8.0 323.4 %all-gather.8.cloned.1.call-start = ((), (), s32[]{:S(2)}) async-start(), calls=%async_computation.1 | async-start | bytes 7208960 | tf_op jit(solution)/shard_map/all_gather | solution.py:25
  8.7 392.7 %all-gather.12.cloned.1.call-start = ((), (), s32[]{:S(2)}) async-start(), calls=%async_computation.3 | async-start | bytes 10485760 | tf_op jit(solution)/shard_map/all_gather | solution.py:8
Sparse Core Ops, SparseCore 0:
  8.9 109.3 all-gather.5
  119.9 104.9 all-gather.9
  226.5 104.9 all-gather.7
  344.9 56.5 all-gather.11

commit v2 on v0

--- a/solution.py
+++ b/solution.py
@@ -2,6 +2,11 @@
 import jax.numpy as jnp
 from jax import lax
 from jax.sharding import PartitionSpec as P
+
+
+def stack_and_merge(x, mesh_axis, along):
+    blocks = lax.all_gather(x, mesh_axis)
+    return jnp.concatenate(blocks, axis=along)
 
 
 def add_rows(left, piece):
@@ -20,9 +25,7 @@
     up = add_one(lax.all_gather(up_weight, "fs", axis=0, tiled=True))
     hidden = (jax.nn.silu(gate) * up).astype(jnp.bfloat16)
     partial_value = jnp.dot(
-        hidden,
-        lax.all_gather(down_weight, "fs", axis=1, tiled=True),
-        preferred_element_type=jnp.float32,
+        hidden, stack_and_merge(down_weight, "fs", 1), preferred_element_type=jnp.float32
     )
     return lax.psum(partial_value.astype(jnp.bfloat16), "tp")
 

time: 404 us -> 405 us (level)
  local copies, waits for them, and re-layouts: 3.17 us -> 11.6 us
  waiting for transfers between devices: 366 us -> 358 us
    all_gather x1, waiting for transfers between devices: 109 us -> 98.1 us  [per_device(): gate = add_one(lax.all_gather(gate_weight, 'fs', axis=0, tiled=True))]
    reshape x0 -> x1, local copies, waits for them, and re-layouts: none -> 8.46 us  [stack_and_merge(): return jnp.concatenate(blocks, axis=along)]
  transfers between devices with their start and end apart: 4 -> 4, of which waited for: 4 -> 4; matrix products, arithmetic and copies ran while one was open for 2% -> 4% of each run, Pallas kernels for 0% -> 0%
where the time goes in v2:
time: 405 us; the launch traced here: 404 us
  waiting for transfers between devices  358 us (88%)
  matrix products  20.9 us (5%)
  between operations  13.1 us (3%)
  local copies, waits for them, and re-layouts  11.6 us (3%)
    all_gather x1, waiting for transfers between devices, stack_and_merge(): blocks = lax.all_gather(x, mesh_axis)  109 us
    all_gather x1, waiting for transfers between devices, per_device(): up = add_one(lax.all_gather(up_weight, 'fs', axis=0, tiled=True))  98.9 us
    all_gather x1, waiting for transfers between devices, per_device(): gate = add_one(lax.all_gather(gate_weight, 'fs', axis=0, tiled=True))  98.1 us
    psum x1, waiting for transfers between devices, per_device(): return lax.psum(partial_value.astype(jnp.bfloat16), 'tp')  49.8 us
    dot_general x1, matrix products, per_device(): jnp.dot(hidden, stack_and_merge(down_weight, 'fs', 1), preferred_element_...  13.3 us
    reshape x1, local copies, waits for them, and re-layouts, stack_and_merge(): return jnp.concatenate(blocks, axis=along)  8.46 us
  transfers between devices with their start and end apart: 4, of which 4 were waited for; matrix products, arithmetic and copies ran while one was open for 4% of the time, Pallas kernels for 0%

profile of v2, /device:TPU:0, one launch (start us, length us, event | category | flops | bytes accessed | tf_op | source)
XLA Modules:
  0.0 404.2 jit_solution(311619322179481045)
XLA Ops:
  6.5 0.0 copy-start
  6.5 0.0 all-gather.9.cloned.1.call-start
  6.5 0.7 all-gather.9.cloned.1.call-update
  7.3 0.0 all-gather.5.cloned.1.call-start
  7.3 0.7 all-gather.5.cloned.1.call-update
  8.0 0.0 all-gather.7.cloned.1.call-start
  8.1 0.7 all-gather.7.cloned.1.call-update
  8.7 0.0 all-reduce.2.cloned.1.call-start
  8.8 0.0 copy-done
  8.8 0.5 fusion
  9.3 109.1 %all-gather.9.cloned.1.call-done = bf16[5632,512]{1,0:T(8,128)(2,1)} async-done(((bf16[1408,512]{1,0:T(8,128)(2,1)}), bf16[5632,512]{1,0:T(8,128)(2,1)}) %all-gather.9.cloned.1.call-update) | async-done | bytes 5767184 | tf_op jit(solution)/shard_map/all_gather | solution.py:8
  118.3 0.0 copy-start.1
  118.3 8.5 %copy.6 = bf16[1408,4,512]{0,2,1:T(8,128)(2,1)} copy(bf16[1408,4,512]{2,0,1:T(8,128)(2,1)} %bitcast.7) | data formatting | bytes 11534336 | tf_op jit(solution)/shard_map/reshape | solution.py:9
  126.8 98.1 %all-gather.5.cloned.1.call-done = bf16[2048,1408]{1,0:T(8,128)(2,1)} async-done(((bf16[512,1408]{1,0:T(8,128)(2,1)}), bf16[2048,1408]{1,0:T(8,128)(2,1)}) %all-gather.5.cloned.1.call-update) | async-done | bytes 5767184 | tf_op jit(solution)/shard_map/all_gather | solution.py:24
  224.9 0.0 copy-done.1
  224.9 7.6 %fusion.6 = f32[512,1408]{1,0:T(8,128)} fusion(bf16[2048,1408]{1,0:T(8,128)(2,1)} %all-gather.5.cloned.1.call-done, bf16[512,2048]{1,0:T(8,128)(2,1)S(1)} %copy-done, f32[2048]{0:T(1024)S(1)} %copy-done.1, f32[512]{0:T(512)S(1)} %add_rsqrt_fusion), kind=kOutput, calls=%fused_computation.8 | convolution fusion | flops 2956984320 | bytes 10758144 | tf_op jit(solution)/shard_map/dot_general | solution.py:13
  232.5 98.9 %all-gather.7.cloned.1.call-done = bf16[2048,1408]{1,0:T(8,128)(2,1)} async-done(((bf16[512,1408]{1,0:T(8,128)(2,1)}), bf16[2048,1408]{1,0:T(8,128)(2,1)}) %all-gather.7.cloned.1.call-update) | async-done | bytes 5767184 | tf_op jit(solution)/shard_map/all_gather | solution.py:25
  331.4 13.3 %convolution_convert_fusion = bf16[512,2048]{1,0:T(8,128)(2,1)} fusion(bf16[1408,2048]{0,1:T(8,128)(2,1)} %bitcast.8, bf16[2048,1408]{1,0:T(8,128)(2,1)} %all-gather.7.cloned.1.call-done, f32[512,1408]{1,0:T(8,128)} %fusion.6, bf16[512,2048]{1,0:T(8,128)(2,1)S(1)} %copy-done, f32[2048]{0:T(1024)S(1)} %copy-done.1, f32[512]{0:T(512)S(1)} %add_rsqrt_fusion), kind=kOutput, calls=%fused_computation.7 | convolution fusion | flops 5915148288 | bytes 18622464 | tf_op jit(solution)/shard_map/dot_general | solution.py:27
  344.7 0.0 all-reduce.2.cloned.1.call-update
  344.7 49.8 %all-reduce.2.cloned.1.call-done = bf16[512,2048]{1,0:T(8,128)(2,1)} async-done(((bf16[512,2048]{1,0:T(8,128)(2,1)}), bf16[512,2048]{1,0:T(8,128)(2,1)}) %all-reduce.2.cloned.1.call-update) | async-done | bytes 2097168 | tf_op jit(solution)/shard_map/psum | solution.py:30
  394.5 3.2 copy.8
  (1 shorter events, 0.0 us)
Async XLA Ops:
  6.5 2.3 copy-start
  6.5 111.8 %all-gather.9.cloned.1.call-start = ((), (), s32[]{:S(2)}) async-start(), calls=%async_computation.3 | async-start | bytes 7208960 | tf_op jit(solution)/shard_map/all_gather | solution.py:8
  7.3 217.6 %all-gather.5.cloned.1.call-start = ((), (), s32[]{:S(2)}) async-start(), calls=%async_computation | async-start | bytes 7208960 | tf_op jit(solution)/shard_map/all_gather | solution.py:24
  8.0 323.4 %all-gather.7.cloned.1.call-start = ((), (), s32[]{:S(2)}) async-start(), calls=%async_computation.1 | async-start | bytes 7208960 | tf_op jit(solution)/shard_map/all_gather | solution.py:25
  8.7 385.8 %all-reduce.2.cloned.1.call-start = ((), (), s32[]{:S(2)}) async-start(), calls=%async_computation.2 | async-start | bytes 4194304 | tf_op jit(solution)/shard_map/psum | solution.py:30
  118.3 106.5 %copy-start.1 = (f32[2048]{0:T(1024)S(1)}, f32[2048]{0:T(1024)}, u32[]{:S(2)}) copy-start(f32[2048]{0:T(1024)} %param.6) | copy-start | bytes 24580
Sparse Core Ops, SparseCore 0:
  8.9 109.3 all-gather.8
  119.9 104.9 all-gather.4
  226.5 104.9 all-gather.6
  344.8 49.6 all-reduce.1
